TPU v7x, 32 devices: a whole 2x2x4 slice. The times are simulated.
32 devices in a mesh: tp: 32 (over z, y, x, core).
Axes of the slice: x: 2, y: 2, z: 4, core: 2. Of those that a mesh axis runs over, the one named last changes fastest.
Arguments:
- tokens: bfloat16 [32, 4096], replicated, may hold values from -18 to 18
- norm_gain: float32 [2, 4096], replicated, may hold values from 0.1 to 1.9
- w_gate: bfloat16 [2, 4096, 8192], P(None, None, 'tp'), may hold values from -0.09375 to 0.09375
- w_value: bfloat16 [2, 4096, 8192], P(None, None, 'tp'), may hold values from -0.09375 to 0.09375
- w_write: bfloat16 [2, 4096, 1024], P(None, None, 'tp'), may hold values from -0.09375 to 0.09375
- w_read: bfloat16 [2, 4096, 1024], P(None, None, 'tp'), may hold values from -0.09375 to 0.09375
- w_step: bfloat16 [2, 4096, 128], replicated, may hold values from -0.09375 to 0.09375
- step_bias: float32 [2, 128], replicated, may hold values from -2 to 1
- decay_rate: float32 [2, 128], replicated, may hold values from 0.05 to 3
- skip_gain: float32 [2, 128], replicated, may hold values from 1 to 4
- conv_value_weight: float32 [2, 3, 8192], P(None, None, 'tp'), may hold values from -2.5 to 2.5
- conv_key_weight: float32 [2, 3, 2, 1024], P(None, None, None, 'tp'), may hold values from -2.5 to 2.5
- group_gain: float32 [2, 8192], P(None, 'tp'), may hold values from 0.1 to 1.9
- w_out: bfloat16 [2, 8192, 4096], P(None, 'tp'), may hold values from -0.0625 to 0.0625
- ssm_state: float32 [2, 32, 8192, 128], P(None, None, 'tp'), may hold values from -3 to 3
- conv_value: float32 [2, 32, 2, 8192], P(None, None, None, 'tp'), may hold values from -5 to 5
- conv_key: float32 [2, 32, 2, 2, 1024], P(None, None, None, None, 'tp'), may hold values from -5 to 5
Outputs:
- tokens_out: bfloat16 [32, 4096], replicated
- ssm_state_out: float32 [2, 32, 8192, 128], P(None, None, 'tp')
- conv_value_out: float32 [2, 32, 2, 8192], P(None, None, None, 'tp')
- conv_key_out: float32 [2, 32, 2, 2, 1024], P(None, None, None, None, 'tp')
All inputs are finite; a program needn't handle non-finite values.
Results may differ from a plain program's by a relative error of at most 0.011.
Values may be sent and summed in bfloat16 or wider, within the bound.
A program may use at most 128 MiB of HBM per device.

v0:
```python
import jax
import jax.numpy as jnp
from jax import lax
from jax.experimental import pallas as pl
from jax.experimental.pallas import tpu as pltpu
from jax.sharding import PartitionSpec as P
import functools

D = 4096
HEAD_DIM = 64
GROUPS = 8
STATE = 128
LAYERS = 2
HEADS = 128
GW = 1024


EPS = 1e-06


def per_device(
    tokens,
    norm_gain,
    w_gate,
    w_value,
    w_write,
    w_read,
    w_step,
    step_bias,
    decay_rate,
    skip_gain,
    conv_value_weight,
    conv_key_weight,
    group_gain,
    w_out,
    ssm_state,
    conv_value,
    conv_key,
):
    highest = lax.Precision.HIGHEST
    chan_count = w_gate.shape[2]
    position = lax.axis_index("tp")
    first_chan = position * chan_count
    chan_ids = first_chan + jnp.arange(chan_count, dtype=jnp.int32)
    my_group = first_chan // GW
    head_hot = (
        (chan_ids // HEAD_DIM)[:, None] == jnp.arange(HEADS, dtype=jnp.int32)[None, :]
    ).astype(jnp.float32)
    group_hot = ((chan_ids // GW)[:, None] == jnp.arange(GROUPS, dtype=jnp.int32)[None, :]).astype(
        jnp.float32
    )
    hidden = tokens
    ssm_list = []
    value_list = []
    key_list = []
    for layer in range(LAYERS):
        resid = hidden.astype(jnp.float32)
        inv_scale = lax.rsqrt(jnp.sum(resid * resid, axis=1) / D + EPS)[:, None]
        scaled = (resid * norm_gain[layer]).astype(jnp.bfloat16)

        def project(weight):
            return jnp.dot(scaled, weight[layer], preferred_element_type=jnp.float32) * inv_scale

        gate_in = project(w_gate)
        value_in = project(w_value)
        write_in = project(w_write)
        read_in = project(w_read)
        step_in = project(w_step)
        value_window = jnp.concatenate([conv_value[layer], value_in[:, None, :]], axis=1)
        value_list.append(value_window[:, 1:])
        values = jax.nn.silu(jnp.sum(value_window * conv_value_weight[layer][None], axis=1))
        fresh = jnp.stack([write_in, read_in], axis=1)[:, None]
        key_window = jnp.concatenate([conv_key[layer], fresh], axis=1)
        key_list.append(key_window[:, 1:])
        mixed_keys = jax.nn.silu(jnp.sum(key_window * conv_key_weight[layer][None], axis=1))
        every_group = lax.all_gather(mixed_keys, "tp", axis=2, tiled=True)
        by_entry = every_group.reshape(every_group.shape[0], 2, STATE, GROUPS)
        own_keys = lax.dynamic_slice_in_dim(by_entry, my_group, 1, 3)[..., 0]
        writes = own_keys[:, 0]
        reads = own_keys[:, 1]
        delta = jax.nn.softplus(step_in + step_bias[layer][None])
        decay = jnp.exp(-delta * decay_rate[layer][None])
        delta_chan = jnp.dot(delta, head_hot.T, precision=highest)
        decay_chan = jnp.dot(decay, head_hot.T, precision=highest)
        skip_chan = jnp.dot(skip_gain[layer], head_hot.T, precision=highest)
        state = (
            decay_chan[..., None] * ssm_state[layer]
            + (delta_chan * values)[..., None] * writes[:, None, :]
        )
        ssm_list.append(state)
        read_out = jnp.sum(state * reads[:, None, :], axis=2) + skip_chan[None] * values
        gated = read_out * jax.nn.silu(gate_in)
        squares = jnp.dot(gated * gated, group_hot, precision=highest)
        square_total = lax.psum(squares, "tp")
        group_scale = lax.rsqrt(square_total / GW + EPS)
        scale_chan = jnp.dot(group_scale, group_hot.T, precision=highest)
        normed = (gated * scale_chan * group_gain[layer][None]).astype(jnp.bfloat16)
        partial_out = jnp.dot(normed, w_out[layer], preferred_element_type=jnp.float32)
        update = lax.psum(partial_out, "tp")
        hidden = (resid + update).astype(jnp.bfloat16)
    return (hidden, jnp.stack(ssm_list), jnp.stack(value_list), jnp.stack(key_list))


LANES = 128
TAPS = 3
VMEM = 67043328
BF16 = jnp.bfloat16
F32 = jnp.float32
NT = (((1,), (1,)), ((), ()))


def split3(x):
    high = x.astype(BF16)
    rest = x - high.astype(F32)
    mid = rest.astype(BF16)
    return high, mid, (rest - mid.astype(F32)).astype(BF16)


def select_dot(x, hot):
    rows = x.shape[0]
    parts = jnp.concatenate(split3(x), axis=0)
    out = jnp.dot(parts, hot, preferred_element_type=F32)
    return out[:rows] + out[rows : 2 * rows] + out[2 * rows :]


def silu(v):
    return v / (1.0 + jnp.exp(-v))


def iota(shape, axis):
    return lax.broadcasted_iota(jnp.int32, shape, axis)


def kernel(
    n,
    tokens_hbm,
    gain_hbm,
    wg_hbm,
    wv_hbm,
    ww_hbm,
    wr_hbm,
    ws_hbm,
    bias_hbm,
    rate_hbm,
    skip_hbm,
    cvw_hbm,
    ckw_hbm,
    gg_hbm,
    wo_hbm,
    state_hbm,
    cv_hbm,
    ck_hbm,
    tokens_out,
    state,
    value_out,
    key_out,
    tokens,
    gain,
    wg,
    wv,
    wk,
    ws,
    bias,
    rate,
    skip,
    cvw,
    ckw,
    gg,
    wo,
    cv,
    ck,
    hidden,
    scaled,
    keys_send,
    keys_recv,
    sq_send,
    sq_recv,
    part,
    rs_send,
    rs_recv,
    cols,
    wbuf,
    rbuf,
    qbuf,
    in_small,
    in_big,
    key_ss,
    key_rs,
    sq_ss,
    sq_rs,
    rs_ss,
    rs_rs,
    ag_ss,
    ag_rs,
):
    layers, batch, chans, entries = state.shape
    width = hidden.shape[3]
    depth = tokens.shape[1]
    key_cols = wk.shape[1] // 2
    own_entries = key_cols // GROUPS
    span = 2 * own_entries
    heads = bias.shape[1]
    peers = GW // chans
    me = lax.axis_index("tp")
    my_group = me // peers
    first = my_group * peers
    kstep = 512
    ksteps = depth // kstep

    small_pairs = (
        (tokens_hbm, tokens),
        (gain_hbm, gain),
        (bias_hbm, bias),
        (rate_hbm, rate),
        (skip_hbm, skip),
        (cvw_hbm, cvw),
        (ckw_hbm, ckw),
        (gg_hbm, gg),
        (cv_hbm, cv),
        (ck_hbm, ck),
    )
    small = [pltpu.make_async_copy(a, b, in_small.at[i]) for i, (a, b) in enumerate(small_pairs)]
    big = [
        [
            pltpu.make_async_copy(a.at[l], b.at[l], in_big.at[l, i])
            for i, (a, b) in enumerate(
                (
                    (ww_hbm, wk.at[:, :key_cols]),
                    (wr_hbm, wk.at[:, key_cols:]),
                    (wg_hbm, wg),
                    (wv_hbm, wv),
                    (ws_hbm, ws),
                    (state_hbm, state),
                    (wo_hbm, wo),
                )
            )
        ]
        for l in range(layers)
    ]
    for copy in small[:2] + big[0][:2] + small[2:] + big[0][2:] + big[1]:
        copy.start()

    barrier = pltpu.get_barrier_semaphore()

    def greet(k, carry):
        pl.semaphore_signal(
            barrier,
            inc=1,
            device_id=(lax.rem(me + k, n),),
            device_id_type=pl.DeviceIdType.MESH,
        )
        return carry

    lax.fori_loop(1, n, greet, 0)

    def remote(src, dst, ss, rs, to):
        return pltpu.make_async_remote_copy(
            src_ref=src,
            dst_ref=dst,
            send_sem=ss,
            recv_sem=rs,
            device_id=(to,),
            device_id_type=pl.DeviceIdType.MESH,
        )

    def key_copy(l, k, slot):
        to = lax.rem(me + k, n)
        return remote(
            keys_send.at[l, to // peers], keys_recv.at[l, slot], key_ss.at[l, k], key_rs.at[l, k], to
        )

    def rs_copy(l, k, slot):
        to = lax.rem(me + k, n)
        return remote(rs_send.at[l, to], rs_recv.at[l, slot], rs_ss.at[l, k], rs_rs.at[l, k], to)

    def ag_copy(l, k, slot):
        to = lax.rem(me + k, n)
        return remote(
            hidden.at[l, me], hidden.at[l, slot], ag_ss.at[l, k], ag_rs.at[l, k], to
        )

    buddy = me + 1 - 2 * lax.rem(me, 2)

    def pair_copy(l, k, slot):
        return remote(
            hidden.at[l, slot], hidden.at[l, slot], ag_ss.at[l, k], ag_rs.at[l, k], buddy
        )

    def sq_copy(l, k):
        to = first + lax.rem(me - first + k, peers)
        return remote(
            sq_send.at[l], sq_recv.at[l, k], sq_ss.at[l, k], sq_rs.at[l, k], to
        )

    def each(body):
        def step(k, carry):
            body(k)
            return carry

        lax.fori_loop(1, n, step, 0)

    def halves(body):
        def step(k, carry):
            body(2 * k)
            return carry

        lax.fori_loop(1, n // 2, step, 0)

    def came_from(k):
        return lax.rem(me + n - k, n)

    row = iota((2 * key_cols, key_cols), 0)
    col = iota((2 * key_cols, key_cols), 1)
    source = (row % own_entries) * GROUPS + row // span
    is_read = (row % span) // own_entries
    send_hot = [
        jnp.where((col == source) & (is_read == i), 1.0, 0.0).astype(BF16) for i in range(2)
    ]
    row = iota((n * span, 2 * entries), 0)
    col = iota((n * span, 2 * entries), 1)
    target = ((row % span) // own_entries) * entries + (row // span) * own_entries + row % own_entries
    recv_hot = jnp.where(col == target, 1.0, 0.0).astype(BF16)
    row = iota((heads, chans), 0)
    col = iota((heads, chans), 1)
    head_hot = jnp.where(row == (me * chans + col) // HEAD_DIM, 1.0, 0.0).astype(BF16)

    def update_state(l, group):
        turned = pltpu.roll(cols[...], lax.rem(LANES - 8 * group, LANES), 1)
        writes8 = wbuf[pl.ds(pl.multiple_of(8 * group, 8), 8), :]
        for j in range(8):
            b = 8 * group + j
            state[l, b] = (
                turned[:, batch + j : batch + j + 1] * state[l, b]
                + turned[:, j : j + 1] * writes8[j : j + 1, :]
            )

    groups8 = batch // 8

    def update_range(l, low, high):
        def step(g, carry):
            update_state(l, g)
            return carry

        lax.fori_loop(low, high, step, 0)

    for copy in small[:2]:
        copy.wait()

    for l in range(layers):
        if l == 0:
            def piece(j):
                return tokens[:, j * width : (j + 1) * width]
        else:
            def piece(j):
                return hidden[l - 1, j]
        squares = jnp.zeros((batch, width), F32)
        for j in range(n):
            x = piece(j).astype(F32)
            squares = squares + x * x
            scaled[:, j * width : (j + 1) * width] = (
                x * gain[l : l + 1, j * width : (j + 1) * width]
            ).astype(BF16)
        inv_scale = lax.rsqrt(jnp.sum(squares, axis=1, keepdims=True) / depth + EPS)

        def project(refs):
            def step(k, accs):
                at = pl.ds(pl.multiple_of(k * kstep, kstep), kstep)
                x = scaled[:, at]
                return tuple(
                    acc + jnp.dot(x, ref[l, at, :], preferred_element_type=F32)
                    for acc, ref in zip(accs, refs)
                )

            zeros = tuple(jnp.zeros((batch, ref.shape[2]), F32) for ref in refs)
            return [acc * inv_scale for acc in lax.fori_loop(0, ksteps, step, zeros)]

        big[l][0].wait()
        big[l][1].wait()
        def key_step(k, acc):
            at = pl.ds(pl.multiple_of(k * kstep, kstep), kstep)
            return acc + lax.dot_general(
                scaled[:, at], wk[l, :, at], NT, preferred_element_type=F32
            )

        key_in = lax.fori_loop(0, ksteps, key_step, jnp.zeros((batch, 2 * key_cols), F32))
        key_in = key_in * inv_scale
        write_in = key_in[:, :key_cols]
        read_in = key_in[:, key_cols:]
        if l == 0:
            for copy in small[2:]:
                copy.wait()
        for i, fresh in enumerate((write_in, read_in)):
            for k in range(1, TAPS - 1):
                key_out[l, :, k - 1, i, :] = ck[l, :, k, i, :]
            key_out[l, :, TAPS - 2, i, :] = fresh
        keys_t = jnp.zeros((2 * key_cols, LANES), F32)
        for i, fresh in enumerate((write_in, read_in)):
            mixed = fresh * ckw[l, TAPS - 1, i : i + 1, :]
            for k in range(TAPS - 1):
                mixed = mixed + ck[l, :, k, i, :] * ckw[l, k, i : i + 1, :]
            mixed = jnp.concatenate(
                [silu(mixed), jnp.zeros((LANES - batch, key_cols), F32)], axis=0
            )
            for p in split3(mixed):
                keys_t = keys_t + lax.dot_general(
                    send_hot[i], p, NT, preferred_element_type=F32
                )
        keys_send[l] = keys_t.reshape(GROUPS, span, LANES)
        keys_recv[l, me] = keys_send[l, my_group]
        if l == 0:
            pl.semaphore_wait(barrier, n - 1)
        each(lambda k: key_copy(l, k, me).start())

        big[l][2].wait()
        big[l][3].wait()
        big[l][4].wait()
        gate_in, value_in, step_in = project((wg, wv, ws))
        for k in range(1, TAPS - 1):
            value_out[l, :, k - 1, :] = cv[l, :, k, :]
        value_out[l, :, TAPS - 2, :] = value_in
        values = value_in * cvw[TAPS - 1, l : l + 1, :]
        for k in range(TAPS - 1):
            values = values + cv[l, :, k, :] * cvw[k, l : l + 1, :]
        values = silu(values)
        raw = step_in + bias[l : l + 1, :]
        delta = jnp.maximum(raw, 0.0) + jnp.log1p(jnp.exp(-jnp.abs(raw)))
        decay = jnp.exp(-delta * rate[l : l + 1, :])
        skips = jnp.broadcast_to(skip[l : l + 1, :], (8, heads))
        chan = select_dot(jnp.concatenate([delta, decay, skips], axis=0), head_hot)
        decay_chan = chan[batch : 2 * batch]
        skip_chan = chan[2 * batch : 2 * batch + 1]
        dv = chan[:batch] * values
        cols[...] = jnp.concatenate(
            [dv, decay_chan, jnp.zeros((LANES - 2 * batch, chans), F32)], axis=0
        ).T
        gate = silu(gate_in)
        big[l][5].wait()

        each(lambda k: key_copy(l, k, came_from(k)).wait_recv())
        arrived = keys_recv[l].reshape(n * span, LANES).T[:batch]
        both = select_dot(arrived, recv_hot)
        writes = both[:, :entries]
        reads = both[:, entries:]
        wbuf[...] = writes
        rbuf[...] = reads
        lane_half = iota((8, 2 * entries), 1) // entries
        sub = iota((8, 2 * entries), 0)

        def query(g, carry):
            at = pl.ds(pl.multiple_of(8 * g, 8), 8)
            reads8 = rbuf[at, :]
            twice = jnp.concatenate([reads8, reads8], axis=1)
            total = jnp.zeros((8, chans), F32)
            for p in range(4):
                left = jnp.where(sub == 2 * p + lane_half, twice, 0.0).astype(BF16)
                right = jnp.concatenate(
                    [state[l, 8 * g + 2 * p], state[l, 8 * g + 2 * p + 1]], axis=1
                ).astype(BF16)
                total = total + lax.dot_general(left, right, NT, preferred_element_type=F32)
            qbuf[at, :] = total
            return carry

        lax.fori_loop(0, groups8, query, 0)
        through = jnp.sum(writes * reads, axis=1, keepdims=True)
        mixed_out = decay_chan * qbuf[...] + dv * through + skip_chan * values
        gated = mixed_out * gate
        sq_send[l] = jnp.broadcast_to(
            jnp.sum(gated * gated, axis=1, keepdims=True), (batch, LANES)
        )
        for k in range(1, peers):
            sq_copy(l, k).start()
        fed = (gated * gg[l : l + 1, :]).astype(BF16)
        big[l][6].wait()
        per = 4

        def out_step(t, carry):
            res = jnp.dot(
                fed,
                wo[l, :, pl.ds(pl.multiple_of(t * per * width, per * width), per * width)],
                preferred_element_type=F32,
            )
            for i in range(per):
                part[t * per + i] = res[:, i * width : (i + 1) * width]
            return carry

        lax.fori_loop(0, n // per, out_step, 0)
        for k in range(1, peers):
            sq_copy(l, k).wait_recv()
        total = sq_send[l]
        for k in range(1, peers):
            total = total + sq_recv[l, k]
        scale = lax.rsqrt(total / GW + EPS)
        for j in range(n):
            rs_send[l, j] = (part[j] * scale[:, :width]).astype(BF16)
        each(lambda k: rs_copy(l, k, me).start())
        update_range(l, 0, groups8 // 2)
        own = part[me] * scale[:, :width]
        if l == 0:
            resid = tokens[:, pl.ds(pl.multiple_of(me * width, width), width)]
        else:
            resid = hidden[l - 1, me]
        each(lambda k: rs_copy(l, k, came_from(k)).wait_recv())
        rs_recv[l, me] = jnp.zeros((batch, width), BF16)
        sums = [own, jnp.zeros_like(own), jnp.zeros_like(own), jnp.zeros_like(own)]
        for j in range(n):
            sums[j % 4] = sums[j % 4] + rs_recv[l, j].astype(F32)
        update = (sums[0] + sums[1]) + (sums[2] + sums[3])
        hidden[l, me] = (resid.astype(F32) + update).astype(BF16)
        pair_copy(l, 1, me).start()
        halves(lambda k: ag_copy(l, k, me).start())
        update_range(l, groups8 // 2, groups8)

        def forward(k):
            ag_copy(l, k, came_from(k)).wait_recv()
            pair_copy(l, k + 1, came_from(k)).start()

        halves(forward)
        pair_copy(l, 1, buddy).wait_recv()
        halves(lambda k: pair_copy(l, k + 1, lax.rem(buddy + n - k, n)).wait_recv())

    for j in range(n):
        tokens_out[:, j * width : (j + 1) * width] = hidden[layers - 1, j]
    for l in range(layers):
        def drain(k):
            key_copy(l, k, me).wait_send()
            rs_copy(l, k, me).wait_send()

        each(drain)
        pair_copy(l, 1, me).wait_send()

        def drain_pair(k):
            ag_copy(l, k, me).wait_send()
            pair_copy(l, k + 1, came_from(k)).wait_send()

        halves(drain_pair)
        for k in range(1, peers):
            sq_copy(l, k).wait_send()


def fused(n, *args):
    (tokens, norm_gain, w_gate, w_value, w_write, w_read, w_step, step_bias, decay_rate) = args[:9]
    (skip_gain, cvw, ckw, group_gain, w_out, ssm_state, conv_value, conv_key) = args[9:]
    layers, batch, chans, entries = ssm_state.shape
    depth = tokens.shape[1]
    key_cols = w_write.shape[2]
    peers = GW // chans
    span = 2 * (key_cols // GROUPS)
    width = depth // n
    operands = list(args)
    operands[4] = jnp.swapaxes(w_write, 1, 2)
    operands[5] = jnp.swapaxes(w_read, 1, 2)
    operands[10] = jnp.swapaxes(cvw, 0, 1)
    landed = [pltpu.VMEM(a.shape, a.dtype) for a in operands]
    landed[4:6] = [pltpu.VMEM((layers, 2 * key_cols, depth), BF16)]
    del landed[13]
    dma = pltpu.SemaphoreType.DMA
    hidden, state, value_state, key_state = pl.pallas_call(
        functools.partial(kernel, n),
        out_shape=(
            jax.ShapeDtypeStruct(tokens.shape, BF16),
            pltpu.VMEM(ssm_state.shape, F32),
            jax.ShapeDtypeStruct(conv_value.shape, F32),
            jax.ShapeDtypeStruct(conv_key.shape, F32),
        ),
        in_specs=[pl.BlockSpec(memory_space=pltpu.HBM)] * len(operands),
        out_specs=(
            pl.BlockSpec(memory_space=pltpu.VMEM),
            pl.BlockSpec(memory_space=pltpu.VMEM),
            pl.BlockSpec(memory_space=pltpu.VMEM),
            pl.BlockSpec(memory_space=pltpu.VMEM),
        ),
        scratch_shapes=landed
        + [
            pltpu.VMEM((layers, n, batch, width), BF16),
            pltpu.VMEM((batch, depth), BF16),
            pltpu.VMEM((layers, GROUPS, span, LANES), F32),
            pltpu.VMEM((layers, n, span, LANES), F32),
            pltpu.VMEM((layers, batch, LANES), F32),
            pltpu.VMEM((layers, peers, batch, LANES), F32),
            pltpu.VMEM((n, batch, width), F32),
            pltpu.VMEM((layers, n, batch, width), BF16),
            pltpu.VMEM((layers, n, batch, width), BF16),
            pltpu.VMEM((chans, LANES), F32),
            pltpu.VMEM((batch, entries), F32),
            pltpu.VMEM((batch, entries), F32),
            pltpu.VMEM((batch, chans), F32),
            dma((10,)),
            dma((layers, 7)),
            dma((layers, n)),
            dma((layers, n)),
            dma((layers, peers)),
            dma((layers, peers)),
            dma((layers, n)),
            dma((layers, n)),
            dma((layers, n)),
            dma((layers, n)),
        ],
        compiler_params=pltpu.CompilerParams(
            collective_id=0, has_side_effects=True, vmem_limit_bytes=VMEM - ssm_state.size * 4 - 768 * 1024
        ),
        name="mixer",
    )(*operands)
    return hidden, state, value_state, key_state


def dispatch(n, *args):
    depth = args[0].shape[1]
    batch, chans = args[14].shape[1:3]
    own_entries = args[4].shape[2] // GROUPS
    fits = (
        depth == n * LANES
        and 2 * own_entries == 8
        and chans % LANES == 0
        and GW % chans == 0
        and 2 * batch <= LANES
        and batch % 16 == 0
        and n % 2 == 0
    )
    return fused(n, *args) if fits else per_device(*args)


def solution(mesh):
    placed = (
        P(),
        P(),
        P(None, None, "tp"),
        P(None, None, "tp"),
        P(None, None, "tp"),
        P(None, None, "tp"),
        P(),
        P(),
        P(),
        P(),
        P(None, None, "tp"),
        P(None, None, None, "tp"),
        P(None, "tp"),
        P(None, "tp", None),
        P(None, None, "tp", None),
        P(None, None, None, "tp"),
        P(None, None, None, None, "tp"),
    )
    return jax.shard_map(
        functools.partial(dispatch, mesh.shape["tp"]),
        mesh=mesh,
        in_specs=placed,
        out_specs=(
            P(),
            P(None, None, "tp", None),
            P(None, None, None, "tp"),
            P(None, None, None, None, "tp"),
        ),
        check_vma=False,
    )
```

profile of v0, /device:TPU:0, one launch (start us, length us, event | category | flops | bytes accessed | tf_op | source)
XLA Modules:
  0.0 71.9 jit_solution(10906734361440390479)
XLA Ops:
  0.6 65.8 %mixer.1 = (bf16[32,4096]{1,0:T(8,128)(2,1)}, f32[2,32,256,128]{3,2,1,0:T(8,128)S(1)}, f32[2,32,2,256]{3,2,1,0:T(2,128)}, f32[2,32,2,2,32]{4,3,2,1,0:T(2,128)}) custom-call(bf16[32,4096]{1,0:T(8,128)(2,1)} %tokens_hbm.1, f32[2,4096]{1,0:T(2,128)} %gain_hbm.1, bf16[2,4096,256]{2,1,0:T(8,128)(2,1)} %wg_hbm.1, bf16[2,4096,256]{2,1,0:T(8,128)(2,1)} %wv_hbm.1, ...), custom_call_target="tpu_custom_call" | custom-call | tf_op jit(solution)/shard_map/mixer/pallas_call | solution.py:557
  66.5 0.0 copy-start
  66.5 0.0 copy-start.2
  66.5 0.0 copy-start.1
  66.5 3.4 %copy.25 = f32[2,32,256,128]{3,2,1,0:T(8,128)} copy(f32[2,32,256,128]{3,2,1,0:T(8,128)S(1)} %get-tuple-element.5) | data formatting | bytes 16777216
  69.9 0.0 copy-done
  69.9 0.7 copy.26
  70.6 0.0 copy-done.2
  70.6 0.7 copy.27
  71.2 0.0 copy-done.1
  71.3 0.7 copy.28
Async XLA Ops:
  66.5 3.4 %copy-start = (bf16[32,4096]{1,0:T(8,128)(2,1)S(1)}, bf16[32,4096]{1,0:T(8,128)(2,1)}, u32[]{:S(2)}) copy-start(bf16[32,4096]{1,0:T(8,128)(2,1)} %get-tuple-element.12) | copy-start | bytes 786436
  66.5 4.1 %copy-start.2 = (f32[2,32,2,256]{3,2,1,0:T(2,128)S(1)}, f32[2,32,2,256]{3,2,1,0:T(2,128)}, u32[]{:S(2)}) copy-start(f32[2,32,2,256]{3,2,1,0:T(2,128)} %get-tuple-element.14) | copy-start | bytes 393220
  66.5 4.8 %copy-start.1 = (f32[2,32,2,2,32]{4,3,2,1,0:T(2,128)S(1)}, f32[2,32,2,2,32]{4,3,2,1,0:T(2,128)}, u32[]{:S(2)}) copy-start(f32[2,32,2,2,32]{4,3,2,1,0:T(2,128)} %get-tuple-element.15) | copy-start | bytes 98308
where the time goes:
time: 72.7 us; the launch traced here: 71.9 us
  Pallas kernels  65.8 us (91%)
  local copies, waits for them, and re-layouts  5.43 us (7%)
    pallas_call x1, Pallas kernels, fused(): pl.pallas_call(functools.partial(kernel, n), out_shape=(jax.ShapeDtypeStr...  65.8 us
    unnamed x10, local copies, waits for them, and re-layouts  5.43 us

commit v1 on v0

v1 whole, which is shorter than its diff:
```python
import jax
import jax.numpy as jnp
from jax import lax
from jax.experimental import pallas as pl
from jax.experimental.pallas import tpu as pltpu
from jax.sharding import PartitionSpec as P
import functools

D = 4096
HEAD_DIM = 64
GROUPS = 8
STATE = 128
LAYERS = 2
HEADS = 128
GW = 1024


EPS = 1e-06


def per_device(
    tokens,
    norm_gain,
    w_gate,
    w_value,
    w_write,
    w_read,
    w_step,
    step_bias,
    decay_rate,
    skip_gain,
    conv_value_weight,
    conv_key_weight,
    group_gain,
    w_out,
    ssm_state,
    conv_value,
    conv_key,
):
    highest = lax.Precision.HIGHEST
    chan_count = w_gate.shape[2]
    position = lax.axis_index("tp")
    first_chan = position * chan_count
    chan_ids = first_chan + jnp.arange(chan_count, dtype=jnp.int32)
    my_group = first_chan // GW
    head_hot = (
        (chan_ids // HEAD_DIM)[:, None] == jnp.arange(HEADS, dtype=jnp.int32)[None, :]
    ).astype(jnp.float32)
    group_hot = ((chan_ids // GW)[:, None] == jnp.arange(GROUPS, dtype=jnp.int32)[None, :]).astype(
        jnp.float32
    )
    hidden = tokens
    ssm_list = []
    value_list = []
    key_list = []
    for layer in range(LAYERS):
        resid = hidden.astype(jnp.float32)
        inv_scale = lax.rsqrt(jnp.sum(resid * resid, axis=1) / D + EPS)[:, None]
        scaled = (resid * norm_gain[layer]).astype(jnp.bfloat16)

        def project(weight):
            return jnp.dot(scaled, weight[layer], preferred_element_type=jnp.float32) * inv_scale

        gate_in = project(w_gate)
        value_in = project(w_value)
        write_in = project(w_write)
        read_in = project(w_read)
        step_in = project(w_step)
        value_window = jnp.concatenate([conv_value[layer], value_in[:, None, :]], axis=1)
        value_list.append(value_window[:, 1:])
        values = jax.nn.silu(jnp.sum(value_window * conv_value_weight[layer][None], axis=1))
        fresh = jnp.stack([write_in, read_in], axis=1)[:, None]
        key_window = jnp.concatenate([conv_key[layer], fresh], axis=1)
        key_list.append(key_window[:, 1:])
        mixed_keys = jax.nn.silu(jnp.sum(key_window * conv_key_weight[layer][None], axis=1))
        every_group = lax.all_gather(mixed_keys, "tp", axis=2, tiled=True)
        by_entry = every_group.reshape(every_group.shape[0], 2, STATE, GROUPS)
        own_keys = lax.dynamic_slice_in_dim(by_entry, my_group, 1, 3)[..., 0]
        writes = own_keys[:, 0]
        reads = own_keys[:, 1]
        delta = jax.nn.softplus(step_in + step_bias[layer][None])
        decay = jnp.exp(-delta * decay_rate[layer][None])
        delta_chan = jnp.dot(delta, head_hot.T, precision=highest)
        decay_chan = jnp.dot(decay, head_hot.T, precision=highest)
        skip_chan = jnp.dot(skip_gain[layer], head_hot.T, precision=highest)
        state = (
            decay_chan[..., None] * ssm_state[layer]
            + (delta_chan * values)[..., None] * writes[:, None, :]
        )
        ssm_list.append(state)
        read_out = jnp.sum(state * reads[:, None, :], axis=2) + skip_chan[None] * values
        gated = read_out * jax.nn.silu(gate_in)
        squares = jnp.dot(gated * gated, group_hot, precision=highest)
        square_total = lax.psum(squares, "tp")
        group_scale = lax.rsqrt(square_total / GW + EPS)
        scale_chan = jnp.dot(group_scale, group_hot.T, precision=highest)
        normed = (gated * scale_chan * group_gain[layer][None]).astype(jnp.bfloat16)
        partial_out = jnp.dot(normed, w_out[layer], preferred_element_type=jnp.float32)
        update = lax.psum(partial_out, "tp")
        hidden = (resid + update).astype(jnp.bfloat16)
    return (hidden, jnp.stack(ssm_list), jnp.stack(value_list), jnp.stack(key_list))


LANES = 128
TAPS = 3
VMEM = 67043328
BF16 = jnp.bfloat16
F32 = jnp.float32
NT = (((1,), (1,)), ((), ()))


def split3(x):
    high = x.astype(BF16)
    rest = x - high.astype(F32)
    mid = rest.astype(BF16)
    return high, mid, (rest - mid.astype(F32)).astype(BF16)


def select_dot(x, hot):
    rows = x.shape[0]
    parts = jnp.concatenate(split3(x), axis=0)
    out = jnp.dot(parts, hot, preferred_element_type=F32)
    return out[:rows] + out[rows : 2 * rows] + out[2 * rows :]


def silu(v):
    return v / (1.0 + jnp.exp(-v))


def iota(shape, axis):
    return lax.broadcasted_iota(jnp.int32, shape, axis)


def mixer(
    n,
    tokens_hbm,
    gain_hbm,
    wg_hbm,
    wv_hbm,
    ww_hbm,
    wr_hbm,
    ws_hbm,
    bias_hbm,
    rate_hbm,
    skip_hbm,
    cvw_hbm,
    ckw_hbm,
    gg_hbm,
    wo_hbm,
    state_hbm,
    cv_hbm,
    ck_hbm,
    tokens_out,
    state,
    value_out,
    key_out,
    tokens,
    gain,
    wg,
    wv,
    wk,
    ws,
    bias,
    rate,
    skip,
    cvw,
    ckw,
    gg,
    wo,
    cv,
    ck,
    hidden,
    scaled,
    keys_send,
    keys_recv,
    pair_send,
    pair_recv,
    part,
    rs_send,
    rs_recv,
    sq_own,
    sq_pair,
    sq_send,
    sq_recv,
    scales,
    turned,
    cols,
    wbuf,
    in_small,
    in_big,
    key_ss,
    key_rs,
    pair_ss,
    pair_rs,
    sp_ss,
    sp_rs,
    sq_ss,
    sq_rs,
    rs_ss,
    rs_rs,
    ag_ss,
    ag_rs,
    fw_ss,
    fw_rs,
):
    layers, batch, chans, entries = state.shape
    depth = tokens.shape[1]
    chips = n // 2
    block = depth // chips
    key_cols = wk.shape[1] // 2
    own_entries = key_cols // GROUPS
    heads = bias.shape[1]
    peers = GW // chans
    per_group = peers // 2
    me = lax.axis_index("tp")
    chip = me // 2
    core = lax.rem(me, 2)
    other = 1 - core
    buddy = 2 * chip + other
    my_group = me // peers

    small_pairs = (
        (tokens_hbm, tokens),
        (gain_hbm, gain),
        (ck_hbm, ck),
        (ckw_hbm, ckw),
        (bias_hbm, bias),
        (rate_hbm, rate),
        (skip_hbm, skip),
        (cvw_hbm, cvw),
        (gg_hbm, gg),
        (cv_hbm, cv),
    )
    small = [pltpu.make_async_copy(a, b, in_small.at[i]) for i, (a, b) in enumerate(small_pairs)]
    big = [
        [
            pltpu.make_async_copy(a.at[l], b.at[l], in_big.at[l, i])
            for i, (a, b) in enumerate(
                (
                    (ww_hbm, wk.at[:, :key_cols]),
                    (wr_hbm, wk.at[:, key_cols:]),
                    (wg_hbm, wg),
                    (wv_hbm, wv),
                    (ws_hbm, ws),
                    (state_hbm, state),
                    (wo_hbm, wo),
                )
            )
        ]
        for l in range(layers)
    ]
    for copy in small[:4] + big[0][:2]:
        copy.start()

    def flipped(value, mask):
        bit = 1
        out = value
        while bit <= mask:
            if mask & bit:
                out = out + bit - 2 * bit * lax.rem(value // bit, 2)
            bit *= 2
        return out

    chip_of = [flipped(chip, m) for m in range(chips)]

    def distance(m):
        return (m >> 2) + (m >> 1) % 2 + m % 2

    near = sorted(range(chips), key=lambda m: (distance(m), m))
    far = near[::-1]

    barrier = pltpu.get_barrier_semaphore()

    def signal(to):
        pl.semaphore_signal(barrier, inc=1, device_id=(to,), device_id_type=pl.DeviceIdType.MESH)

    for m in far[:-1]:
        signal(2 * chip_of[m])
        signal(2 * chip_of[m] + 1)
    signal(buddy)

    def remote(src, dst, ss, rs, to):
        return pltpu.make_async_remote_copy(
            src_ref=src,
            dst_ref=dst,
            send_sem=ss,
            recv_sem=rs,
            device_id=(to,),
            device_id_type=pl.DeviceIdType.MESH,
        )

    row = iota((2 * LANES, 2 * entries), 0)
    col = iota((2 * LANES, 2 * entries), 1)
    half = row // LANES
    inner = row % LANES
    entry = half * 2 + inner // (LANES // 2)
    sender = (inner % (LANES // 2)) // 2
    recv_hot = jnp.where(
        col == (inner % 2) * entries + sender * own_entries + entry, 1.0, 0.0
    ).astype(BF16)
    row = iota((heads, chans), 0)
    col = iota((heads, chans), 1)
    head_hot = jnp.where(row == (me * chans + col) // HEAD_DIM, 1.0, 0.0).astype(BF16)

    groups8 = batch // 8

    def update_state(l, group):
        shifted = pltpu.roll(cols[...], lax.rem(LANES - 8 * group, LANES), 1)
        writes8 = wbuf[pl.ds(pl.multiple_of(8 * group, 8), 8), :]
        for j in range(8):
            b = 8 * group + j
            state[l, b] = (
                shifted[:, batch + j : batch + j + 1] * state[l, b]
                + shifted[:, j : j + 1] * writes8[j : j + 1, :]
            )

    def update_range(l, low, high):
        def step(g, carry):
            update_state(l, g)
            return carry

        lax.fori_loop(low, high, step, 0)

    def at_chip(c):
        return pl.ds(pl.multiple_of(c * block, block), block)

    def prepare(l, pos, c, squares):
        if l == 0:
            x = tokens[:, at_chip(c)].astype(F32)
        else:
            x = jnp.concatenate([hidden[l - 1, 2 * c], hidden[l - 1, 2 * c + 1]], axis=1).astype(F32)
        scaled[pos] = (x * gain[l : l + 1, at_chip(c)]).astype(BF16)
        return squares + x * x

    def key_dot(l, pos, c, acc):
        return acc + lax.dot_general(
            scaled[pos], wk[l, :, at_chip(c)], NT, preferred_element_type=F32
        )

    def main_dots(l, pos, c, accs):
        return tuple(
            acc + jnp.dot(scaled[pos], ref[l, at_chip(c), :], preferred_element_type=F32)
            for acc, ref in zip(accs, (wg, wv, ws))
        )

    def send_keys(l, key_acc, squares):
        inv_scale = lax.rsqrt(jnp.sum(squares, axis=1, keepdims=True) / depth + EPS)
        key_in = key_acc * inv_scale
        mixed = []
        for i in range(2):
            fresh = key_in[:, i * key_cols : (i + 1) * key_cols]
            total = fresh * ckw[l, TAPS - 1, i : i + 1, :]
            for k in range(TAPS - 1):
                total = total + ck[l, :, k, i, :] * ckw[l, k, i : i + 1, :]
            mixed.append(silu(total))
        mixed = jnp.concatenate(
            mixed + [jnp.zeros((batch, LANES - 2 * key_cols), F32)], axis=1
        )
        spread = jnp.concatenate([mixed] * own_entries, axis=0).T
        lane_entry = iota((GROUPS, LANES), 1) // batch
        for i in range(2):
            packed = jnp.zeros((GROUPS, LANES), F32)
            for e in range(own_entries):
                at = (i * own_entries + e) * GROUPS
                packed = jnp.where(lane_entry == e, spread[at : at + GROUPS], packed)
            keys_send[l, :, i, :] = packed
        keys_recv[l, me] = keys_send[l, my_group]
        if l == 0:
            pl.semaphore_wait(barrier, n - 1)
        for m in far:
            for to in ([2 * chip_of[m], 2 * chip_of[m] + 1] if m else [buddy]):
                remote(
                    keys_send.at[l, to // peers], keys_recv.at[l, me], key_ss.at[l], key_rs.at[l], to
                ).start()
        return inv_scale, key_in

    zeros = tuple(jnp.zeros((batch, ref.shape[2]), F32) for ref in (wg, wv, ws))
    key_zero = jnp.zeros((batch, 2 * key_cols), F32)
    square_zero = jnp.zeros((batch, block), F32)

    def ag_wait(l, m):
        return remote(
            hidden.at[l, 2 * chip_of[m] + other], hidden.at[l, 2 * chip_of[m] + other],
            ag_ss.at[l], ag_rs.at[l, m], buddy,
        )

    def forward(l, m):
        s = 2 * chip_of[m] + other
        return remote(hidden.at[l, s], hidden.at[l, s], fw_ss.at[l], fw_rs.at[l, m], buddy)

    def forward_all(l, masks):
        for m in masks:
            if m:
                ag_wait(l, m).wait_recv()
                forward(l, m).start()

    def whole(l, masks):
        for m in masks:
            if m:
                forward(l, m).wait_recv()
            else:
                ag_wait(l, 0).wait_recv()

    for l in range(layers):
        if l == 0:
            for copy in small[:4] + big[0][:2]:
                copy.wait()
            for copy in big[0][2:5] + small[4:]:
                copy.start()
            squares = square_zero
            key_acc = key_zero
            for c in range(chips):
                squares = prepare(l, c, c, squares)
                key_acc = key_dot(l, c, c, key_acc)
            inv_scale, key_in = send_keys(l, key_acc, squares)
            for copy in big[0][2:5]:
                copy.wait()
            for copy in big[0][5:]:
                copy.start()
            accs = zeros
            for c in range(chips):
                accs = main_dots(l, c, c, accs)
            for copy in small[4:]:
                copy.wait()
        else:
            for copy in big[l][:5]:
                copy.wait()
            quarter = chips // 4
            squares, key_acc, accs = square_zero, key_zero, zeros
            waves = [near[q * quarter : (q + 1) * quarter] for q in range(4)]
            forward_all(l - 1, waves[0])
            forward_all(l - 1, waves[1])
            for q, wave in enumerate(waves):
                whole(l - 1, wave)
                for i, m in enumerate(wave):
                    pos = q * quarter + i
                    squares = prepare(l, pos, chip_of[m], squares)
                    key_acc = key_dot(l, pos, chip_of[m], key_acc)
                if q < 3:
                    for i, m in enumerate(wave):
                        accs = main_dots(l, q * quarter + i, chip_of[m], accs)
                if q < 2:
                    forward_all(l - 1, waves[q + 2])
            inv_scale, key_in = send_keys(l, key_acc, squares)
            for i, m in enumerate(waves[3]):
                accs = main_dots(l, 3 * quarter + i, chip_of[m], accs)
        gate_in, value_in, step_in = [acc * inv_scale for acc in accs]
        for i in range(2):
            for k in range(1, TAPS - 1):
                key_out[l, :, k - 1, i, :] = ck[l, :, k, i, :]
            key_out[l, :, TAPS - 2, i, :] = key_in[:, i * key_cols : (i + 1) * key_cols]
        for k in range(1, TAPS - 1):
            value_out[l, :, k - 1, :] = cv[l, :, k, :]
        value_out[l, :, TAPS - 2, :] = value_in
        values = value_in * cvw[TAPS - 1, l : l + 1, :]
        for k in range(TAPS - 1):
            values = values + cv[l, :, k, :] * cvw[k, l : l + 1, :]
        values = silu(values)
        raw = step_in + bias[l : l + 1, :]
        delta = jnp.maximum(raw, 0.0) + jnp.log1p(jnp.exp(-jnp.abs(raw)))
        decay = jnp.exp(-delta * rate[l : l + 1, :])
        skips = jnp.broadcast_to(skip[l : l + 1, :], (8, heads))
        chan = select_dot(jnp.concatenate([delta, decay, skips], axis=0), head_hot)
        decay_chan = chan[batch : 2 * batch]
        skip_chan = chan[2 * batch : 2 * batch + 1]
        dv = chan[:batch] * values
        cols[...] = jnp.concatenate(
            [dv, decay_chan, jnp.zeros((LANES - 2 * batch, chans), F32)], axis=0
        ).T
        gate = silu(gate_in)
        big[l][5].wait()

        def turn(g, carry):
            for j in range(4):
                turned[4 * g + j] = state[l, 4 * g + j].T.astype(BF16)
            return carry

        lax.fori_loop(0, batch // 4, turn, 0)
        big[l][6].wait()

        remote(
            keys_recv.at[l, pl.ds(0, n - 1)], keys_recv.at[l, pl.ds(0, n - 1)],
            key_ss.at[l], key_rs.at[l], buddy,
        ).wait_recv()
        arrived = keys_recv[l].reshape(2 * n, LANES)
        arrived = jnp.concatenate([arrived, arrived], axis=0).T
        left_half = iota((batch, LANES), 1) < LANES // 2
        pieces = [
            jnp.where(
                left_half,
                arrived[2 * h * batch : (2 * h + 1) * batch],
                arrived[(2 * h + 1) * batch : (2 * h + 2) * batch],
            )
            for h in range(2)
        ]
        both = select_dot(jnp.concatenate(pieces, axis=1), recv_hot)
        writes = both[:, :entries]
        reads = both[:, entries:]
        wbuf[...] = writes
        lane_half = iota((8, 2 * entries), 1) // entries
        sub = iota((8, 2 * entries), 0)
        query = []
        for g in range(groups8):
            reads8 = reads[8 * g : 8 * g + 8]
            twice = jnp.concatenate([reads8, reads8], axis=1)
            total = jnp.zeros((8, chans), F32)
            for p in range(4):
                left = jnp.where(sub == 2 * p + lane_half, twice, 0.0).astype(BF16)
                right = turned[pl.ds(8 * g + 2 * p, 2)].reshape(2 * entries, chans)
                total = total + jnp.dot(left, right, preferred_element_type=F32)
            query.append(total)
        query = jnp.concatenate(query, axis=0)
        through = jnp.sum(writes * reads, axis=1, keepdims=True)
        mixed_out = decay_chan * query + dv * through + skip_chan * values
        gated = mixed_out * gate
        fed = (gated * gg[l : l + 1, :]).astype(BF16)

        def out_pair(i, parity):
            rhs = jnp.concatenate(
                [
                    wo[l, :, pl.ds(pl.multiple_of((2 * chip_of[far[i + j]] + parity) * LANES, LANES), LANES)]
                    for j in range(2)
                ],
                axis=1,
            )
            return jnp.dot(fed, rhs, preferred_element_type=F32)

        quarter = chips // 4

        def pair_copy(q):
            at = pl.ds(q * quarter, quarter)
            return remote(
                pair_send.at[l, at], pair_recv.at[l, at], pair_ss.at[l, q], pair_rs.at[l, q], buddy
            )

        for q in range(4):
            for i in range(q * quarter, (q + 1) * quarter, 2):
                res = out_pair(i, core).astype(BF16)
                pair_send[l, i] = res[:, :LANES]
                pair_send[l, i + 1] = res[:, LANES:]
            pair_copy(q).start()
        square = gated * gated
        square = square[:, :LANES] + square[:, LANES:]
        square = jnp.concatenate([square, jnp.zeros((LANES - batch, LANES), F32)], axis=0).T
        sq_own[l] = jnp.sum(square, axis=0, keepdims=True)
        sp_copy = remote(sq_own.at[l], sq_pair.at[l], sp_ss.at[l], sp_rs.at[l], buddy)
        sp_copy.start()
        for i in range(0, chips, 2):
            res = out_pair(i, other)
            part[i] = res[:, :LANES]
            part[i + 1] = res[:, LANES:]

        def rs_copy(i):
            return remote(
                rs_send.at[l, i], rs_recv.at[l, chip], rs_ss.at[l], rs_rs.at[l], 2 * chip_of[far[i]] + other
            )

        for q in range(4):
            pair_copy(q).wait_recv()
            for i in range(q * quarter, (q + 1) * quarter):
                rs_send[l, i] = (part[i] + pair_recv[l, i].astype(F32)).astype(BF16)
                rs_copy(i).start()
        sp_copy.wait_recv()
        sq_send[l] = sq_own[l] + sq_pair[l]
        for m in far:
            remote(
                sq_send.at[l], sq_recv.at[l, chip], sq_ss.at[l], sq_rs.at[l], 2 * chip_of[m] + other
            ).start()
        if l + 1 < layers:
            for copy in big[l + 1]:
                copy.start()
        update_range(l, 0, groups8)
        remote(sq_recv.at[l], sq_recv.at[l], sq_ss.at[l], sq_rs.at[l], buddy).wait_recv()
        rows = []
        for g in range(GROUPS):
            total = sq_recv[l, per_group * g]
            for k in range(1, per_group):
                total = total + sq_recv[l, per_group * g + k]
            rows.append(total)
        rows = lax.rsqrt(jnp.concatenate(rows, axis=0) / GW + EPS)
        columns = jnp.concatenate([rows, jnp.zeros((LANES - GROUPS, LANES), F32)], axis=0).T
        for g in range(GROUPS):
            scales[g] = jnp.broadcast_to(columns[:batch, g : g + 1], (batch, LANES))
        if l == 0:
            resid = tokens[:, pl.ds(pl.multiple_of(me * LANES, LANES), LANES)]
        else:
            resid = hidden[l - 1, me]
        remote(rs_recv.at[l], rs_recv.at[l], rs_ss.at[l], rs_rs.at[l], buddy).wait_recv()
        sums = [resid.astype(F32)] + [jnp.zeros((batch, LANES), F32)] * 3
        for g in range(GROUPS):
            term = rs_recv[l, per_group * g].astype(F32)
            for k in range(1, per_group):
                term = term + rs_recv[l, per_group * g + k].astype(F32)
            sums[g % 4] = sums[g % 4] + term * scales[g]
        hidden[l, me] = ((sums[0] + sums[1]) + (sums[2] + sums[3])).astype(BF16)
        for m in far:
            remote(
                hidden.at[l, me], hidden.at[l, me], ag_ss.at[l], ag_rs.at[l, m], 2 * chip_of[m] + other
            ).start()

    forward_all(layers - 1, near)
    whole(layers - 1, near)
    for j in range(n):
        tokens_out[:, j * LANES : (j + 1) * LANES] = hidden[layers - 1, j]
    for l in range(layers):
        def sent(src, sem):
            remote(src, src, sem, rs_rs.at[l], buddy).wait_send()

        sent(keys_recv.at[l, pl.ds(0, n - 1)], key_ss.at[l])
        for q in range(4):
            sent(pair_send.at[l, pl.ds(0, chips // 4)], pair_ss.at[l, q])
        sent(sq_own.at[l], sp_ss.at[l])
        sent(sq_recv.at[l], sq_ss.at[l])
        sent(rs_send.at[l], rs_ss.at[l])
        sent(hidden.at[l, pl.ds(0, chips)], ag_ss.at[l])
        sent(hidden.at[l, pl.ds(0, chips - 1)], fw_ss.at[l])


def flush(tokens, state, value, key, tokens_hbm, state_hbm, value_hbm, key_hbm, sems):
    layers, batch = state.shape[:2]
    step = batch // 4
    copies = [
        pltpu.make_async_copy(key, key_hbm, sems.at[0]),
        pltpu.make_async_copy(value, value_hbm, sems.at[1]),
        pltpu.make_async_copy(tokens, tokens_hbm, sems.at[2]),
    ]
    for l in range(layers):
        for i in range(4):
            at = pl.ds(i * step, step)
            copies.append(
                pltpu.make_async_copy(state.at[l, at], state_hbm.at[l, at], sems.at[len(copies)])
            )
    for copy in copies:
        copy.start()
    for copy in copies:
        copy.wait()


def fused(n, *args):
    (tokens, norm_gain, w_gate, w_value, w_write, w_read, w_step, step_bias, decay_rate) = args[:9]
    (skip_gain, cvw, ckw, group_gain, w_out, ssm_state, conv_value, conv_key) = args[9:]
    layers, batch, chans, entries = ssm_state.shape
    depth = tokens.shape[1]
    chips = n // 2
    key_cols = w_write.shape[2]
    operands = list(args)
    operands[4] = jnp.swapaxes(w_write, 1, 2)
    operands[5] = jnp.swapaxes(w_read, 1, 2)
    operands[10] = jnp.swapaxes(cvw, 0, 1)
    landed = [pltpu.VMEM(a.shape, a.dtype) for a in operands]
    landed[4:6] = [pltpu.VMEM((layers, 2 * key_cols, depth), BF16)]
    del landed[13]
    dma = pltpu.SemaphoreType.DMA
    outs = (
        jax.ShapeDtypeStruct(tokens.shape, BF16),
        jax.ShapeDtypeStruct(ssm_state.shape, F32),
        jax.ShapeDtypeStruct(conv_value.shape, F32),
        jax.ShapeDtypeStruct(conv_key.shape, F32),
    )
    small_bytes = 4 * 1024 * 1024
    results = pl.pallas_call(
        functools.partial(mixer, n),
        out_shape=tuple(pltpu.VMEM(o.shape, o.dtype) for o in outs),
        in_specs=[pl.BlockSpec(memory_space=pltpu.HBM)] * len(operands),
        out_specs=(pl.BlockSpec(memory_space=pltpu.VMEM),) * 4,
        scratch_shapes=landed
        + [
            pltpu.VMEM((layers, n, batch, LANES), BF16),
            pltpu.VMEM((chips, batch, depth // chips), BF16),
            pltpu.VMEM((layers, GROUPS, 2, LANES), F32),
            pltpu.VMEM((layers, n, 2, LANES), F32),
            pltpu.VMEM((layers, chips, batch, LANES), BF16),
            pltpu.VMEM((layers, chips, batch, LANES), BF16),
            pltpu.VMEM((chips, batch, LANES), F32),
            pltpu.VMEM((layers, chips, batch, LANES), BF16),
            pltpu.VMEM((layers, chips, batch, LANES), BF16),
            pltpu.VMEM((layers, 1, LANES), F32),
            pltpu.VMEM((layers, 1, LANES), F32),
            pltpu.VMEM((layers, 1, LANES), F32),
            pltpu.VMEM((layers, chips, 1, LANES), F32),
            pltpu.VMEM((GROUPS, batch, LANES), F32),
            pltpu.VMEM((batch, entries, chans), BF16),
            pltpu.VMEM((chans, LANES), F32),
            pltpu.VMEM((batch, entries), F32),
            dma((10,)),
            dma((layers, 7)),
            dma((layers,)),
            dma((layers,)),
            dma((layers, 4)),
            dma((layers, 4)),
            dma((layers,)),
            dma((layers,)),
            dma((layers,)),
            dma((layers,)),
            dma((layers,)),
            dma((layers,)),
            dma((layers,)),
            dma((layers, chips)),
            dma((layers,)),
            dma((layers, chips)),
        ],
        compiler_params=pltpu.CompilerParams(
            collective_id=0,
            has_side_effects=True,
            vmem_limit_bytes=VMEM - ssm_state.size * 4 - small_bytes,
        ),
        name="mixer",
    )(*operands)
    return pl.pallas_call(
        flush,
        out_shape=outs,
        in_specs=[pl.BlockSpec(memory_space=pl.ANY)] * 4,
        out_specs=(pl.BlockSpec(memory_space=pltpu.HBM),) * 4,
        scratch_shapes=[dma((3 + 4 * layers,))],
        compiler_params=pltpu.CompilerParams(vmem_limit_bytes=1024 * 1024),
        name="flush",
    )(*results)


def dispatch(n, *args):
    depth = args[0].shape[1]
    layers, batch, chans, entries = args[14].shape
    own_entries = args[4].shape[2] // GROUPS
    fits = (
        depth == n * LANES
        and n == 32
        and own_entries == 4
        and own_entries * batch == LANES
        and entries == LANES
        and chans == 2 * LANES
        and args[7].shape[1] == LANES
    )
    return fused(n, *args) if fits else per_device(*args)


def solution(mesh):
    placed = (
        P(),
        P(),
        P(None, None, "tp"),
        P(None, None, "tp"),
        P(None, None, "tp"),
        P(None, None, "tp"),
        P(),
        P(),
        P(),
        P(),
        P(None, None, "tp"),
        P(None, None, None, "tp"),
        P(None, "tp"),
        P(None, "tp", None),
        P(None, None, "tp", None),
        P(None, None, None, "tp"),
        P(None, None, None, None, "tp"),
    )
    return jax.shard_map(
        functools.partial(dispatch, mesh.shape["tp"]),
        mesh=mesh,
        in_specs=placed,
        out_specs=(
            P(),
            P(None, None, "tp", None),
            P(None, None, None, "tp"),
            P(None, None, None, None, "tp"),
        ),
        check_vma=False,
    )
```

time: 72.7 us -> 49.2 us (0.68)
  Pallas kernels: 65.8 us -> 48.4 us
  local copies, waits for them, and re-layouts: 5.43 us -> 0 us
    pallas_call x1 -> x2, Pallas kernels: 65.8 us -> 48.4 us  [the longest x1 44.8 us: fused(): pl.pallas_call(functools.partial(mixer, n), out_shape=tuple((pltpu.VMEM(o...]
    unnamed x10 -> x0, local copies, waits for them, and re-layouts: 5.43 us -> none
where the time goes in v1:
time: 49.2 us; the launch traced here: 49 us
  Pallas kernels  48.4 us (98%)
  between operations  0.65 us (1%)
    pallas_call x1, Pallas kernels, fused(): pl.pallas_call(functools.partial(mixer, n), out_shape=tuple((pltpu.VMEM(o...  44.8 us
    pallas_call x1, Pallas kernels, fused(): pl.pallas_call(flush, out_shape=outs, in_specs=[pl.BlockSpec(memory_space...  3.57 us

profile of v1, /device:TPU:0, one launch (start us, length us, event | category | flops | bytes accessed | tf_op | source)
XLA Modules:
  0.0 49.0 jit_solution(7127854143178011194)
XLA Ops:
  0.6 44.8 %mixer.1 = (bf16[32,4096]{1,0:T(8,128)(2,1)S(1)}, f32[2,32,256,128]{3,2,1,0:T(8,128)S(1)}, f32[2,32,2,256]{3,2,1,0:T(2,128)S(1)}, f32[2,32,2,2,32]{4,3,2,1,0:T(2,128)S(1)}) custom-call(bf16[32,4096]{1,0:T(8,128)(2,1)} %tokens_hbm.1, f32[2,4096]{1,0:T(2,128)} %gain_hbm.1, bf16[2,4096,256]{2,1,0:T(8,128)(2,1)} %wg_hbm.1, bf16[2,4096,256]{2,1,0:T(8,128)(2,1)} %wv_hbm.1, ...), custom_call_target="tpu_custom_call" | custom-call | tf_op jit(solution)/shard_map/mixer/pallas_call | solution.py:661
  45.5 3.6 %flush.1 = (bf16[32,4096]{1,0:T(8,128)(2,1)}, f32[2,32,256,128]{3,2,1,0:T(8,128)}, f32[2,32,2,256]{3,2,1,0:T(2,128)}, f32[2,32,2,2,32]{4,3,2,1,0:T(2,128)}) custom-call(bf16[32,4096]{1,0:T(8,128)(2,1)S(1)} %get-tuple-element.8.tokens, f32[2,32,256,128]{3,2,1,0:T(8,128)S(1)} %get-tuple-element.9.state, f32[2,32,2,256]{3,2,1,0:T(2,128)S(1)} %get-tuple-element.10.value, ...), custom_call_target="tpu_custom_call" | custom-call | tf_op jit(solution)/shard_map/flush/pallas_call | solution.py:709

commit v2 on v1

--- a/solution.py
+++ b/solution.py
@@ -186,23 +186,15 @@
     turned,
     cols,
     wbuf,
-    in_small,
-    in_big,
-    key_ss,
-    key_rs,
-    pair_ss,
+    in_sem,
+    send_sem,
+    recv_sem,
     pair_rs,
-    sp_ss,
-    sp_rs,
-    sq_ss,
-    sq_rs,
-    rs_ss,
-    rs_rs,
-    ag_ss,
     ag_rs,
-    fw_ss,
     fw_rs,
 ):
+    key_ss, pair_ss, rs_ss, ag_ss, fw_ss, sp_ss, sq_ss = [send_sem.at[i] for i in range(7)]
+    key_rs, sp_rs, sq_rs, rs_rs = [recv_sem.at[i] for i in range(4)]
     layers, batch, chans, entries = state.shape
     depth = tokens.shape[1]
     chips = n // 2
@@ -231,10 +223,10 @@
         (gg_hbm, gg),
         (cv_hbm, cv),
     )
-    small = [pltpu.make_async_copy(a, b, in_small.at[i]) for i, (a, b) in enumerate(small_pairs)]
+    small = [pltpu.make_async_copy(a, b, in_sem.at[i]) for i, (a, b) in enumerate(small_pairs)]
     big = [
         [
-            pltpu.make_async_copy(a.at[l], b.at[l], in_big.at[l, i])
+            pltpu.make_async_copy(a.at[l], b.at[l], in_sem.at[len(small_pairs) + i])
             for i, (a, b) in enumerate(
                 (
                     (ww_hbm, wk.at[:, :key_cols]),
@@ -370,7 +362,7 @@
         for m in far:
             for to in ([2 * chip_of[m], 2 * chip_of[m] + 1] if m else [buddy]):
                 remote(
-                    keys_send.at[l, to // peers], keys_recv.at[l, me], key_ss.at[l], key_rs.at[l], to
+                    keys_send.at[l, to // peers], keys_recv.at[l, me], key_ss, key_rs, to
                 ).start()
         return inv_scale, key_in
 
@@ -378,45 +370,43 @@
     key_zero = jnp.zeros((batch, 2 * key_cols), F32)
     square_zero = jnp.zeros((batch, block), F32)
 
-    def ag_wait(l, m):
-        return remote(
-            hidden.at[l, 2 * chip_of[m] + other], hidden.at[l, 2 * chip_of[m] + other],
-            ag_ss.at[l], ag_rs.at[l, m], buddy,
-        )
-
-    def forward(l, m):
-        s = 2 * chip_of[m] + other
-        return remote(hidden.at[l, s], hidden.at[l, s], fw_ss.at[l], fw_rs.at[l, m], buddy)
-
-    def forward_all(l, masks):
-        for m in masks:
+    quarter = chips // 4
+    waves = [near[q * quarter : (q + 1) * quarter] for q in range(4)]
+    wave_of = {m: q for q, wave in enumerate(waves) for m in wave}
+
+    def blocks(l, count):
+        return hidden.at[l, pl.ds(0, count)]
+
+    def forward_wave(l, q):
+        remote(blocks(l, quarter), blocks(l, quarter), ag_ss, ag_rs.at[q], buddy).wait_recv()
+        for m in waves[q]:
             if m:
-                ag_wait(l, m).wait_recv()
-                forward(l, m).start()
-
-    def whole(l, masks):
-        for m in masks:
-            if m:
-                forward(l, m).wait_recv()
-            else:
-                ag_wait(l, 0).wait_recv()
+                at = hidden.at[l, 2 * chip_of[m] + other]
+                remote(at, at, fw_ss, fw_rs.at[q], buddy).start()
+
+    def whole(l, q):
+        count = sum(1 for m in waves[q] if m)
+        remote(blocks(l, count), blocks(l, count), fw_ss, fw_rs.at[q], buddy).wait_recv()
+
+    def sent(src, sem):
+        remote(src, src, sem, rs_rs, buddy).wait_send()
 
     for l in range(layers):
         if l == 0:
+            for copy in big[0][2:5] + small[4:]:
+                copy.start()
             for copy in small[:4] + big[0][:2]:
                 copy.wait()
-            for copy in big[0][2:5] + small[4:]:
-                copy.start()
             squares = square_zero
             key_acc = key_zero
             for c in range(chips):
                 squares = prepare(l, c, c, squares)
                 key_acc = key_dot(l, c, c, key_acc)
             inv_scale, key_in = send_keys(l, key_acc, squares)
+            for copy in big[0][5:]:
+                copy.start()
             for copy in big[0][2:5]:
                 copy.wait()
-            for copy in big[0][5:]:
-                copy.start()
             accs = zeros
             for c in range(chips):
                 accs = main_dots(l, c, c, accs)
@@ -425,25 +415,18 @@
         else:
             for copy in big[l][:5]:
                 copy.wait()
-            quarter = chips // 4
             squares, key_acc, accs = square_zero, key_zero, zeros
-            waves = [near[q * quarter : (q + 1) * quarter] for q in range(4)]
-            forward_all(l - 1, waves[0])
-            forward_all(l - 1, waves[1])
+            for q in range(4):
+                forward_wave(l - 1, q)
             for q, wave in enumerate(waves):
-                whole(l - 1, wave)
+                whole(l - 1, q)
                 for i, m in enumerate(wave):
                     pos = q * quarter + i
                     squares = prepare(l, pos, chip_of[m], squares)
                     key_acc = key_dot(l, pos, chip_of[m], key_acc)
-                if q < 3:
-                    for i, m in enumerate(wave):
-                        accs = main_dots(l, q * quarter + i, chip_of[m], accs)
-                if q < 2:
-                    forward_all(l - 1, waves[q + 2])
             inv_scale, key_in = send_keys(l, key_acc, squares)
-            for i, m in enumerate(waves[3]):
-                accs = main_dots(l, 3 * quarter + i, chip_of[m], accs)
+            for pos, m in enumerate(near):
+                accs = main_dots(l, pos, chip_of[m], accs)
         gate_in, value_in, step_in = [acc * inv_scale for acc in accs]
         for i in range(2):
             for k in range(1, TAPS - 1):
@@ -469,6 +452,10 @@
         ).T
         gate = silu(gate_in)
         big[l][5].wait()
+        if l:
+            sent(rs_send.at[l - 1], rs_ss)
+            sent(blocks(l - 1, chips), ag_ss)
+            sent(blocks(l - 1, chips - 1), fw_ss)
 
         def turn(g, carry):
             for j in range(4):
@@ -480,7 +467,7 @@
 
         remote(
             keys_recv.at[l, pl.ds(0, n - 1)], keys_recv.at[l, pl.ds(0, n - 1)],
-            key_ss.at[l], key_rs.at[l], buddy,
+            key_ss, key_rs, buddy,
         ).wait_recv()
         arrived = keys_recv[l].reshape(2 * n, LANES)
         arrived = jnp.concatenate([arrived, arrived], axis=0).T
@@ -525,13 +512,16 @@
             )
             return jnp.dot(fed, rhs, preferred_element_type=F32)
 
-        quarter = chips // 4
+        square = gated * gated
+        square = square[:, :LANES] + square[:, LANES:]
+        square = jnp.concatenate([square, jnp.zeros((LANES - batch, LANES), F32)], axis=0).T
+        sq_own[l] = jnp.sum(square, axis=0, keepdims=True)
+        sp_copy = remote(sq_own.at[l], sq_pair.at[l], sp_ss, sp_rs, buddy)
+        sp_copy.start()
 
         def pair_copy(q):
             at = pl.ds(q * quarter, quarter)
-            return remote(
-                pair_send.at[l, at], pair_recv.at[l, at], pair_ss.at[l, q], pair_rs.at[l, q], buddy
-            )
+            return remote(pair_send.at[l, at], pair_recv.at[l, at], pair_ss, pair_rs.at[q], buddy)
 
         for q in range(4):
             for i in range(q * quarter, (q + 1) * quarter, 2):
@@ -539,20 +529,20 @@
                 pair_send[l, i] = res[:, :LANES]
                 pair_send[l, i + 1] = res[:, LANES:]
             pair_copy(q).start()
-        square = gated * gated
-        square = square[:, :LANES] + square[:, LANES:]
-        square = jnp.concatenate([square, jnp.zeros((LANES - batch, LANES), F32)], axis=0).T
-        sq_own[l] = jnp.sum(square, axis=0, keepdims=True)
-        sp_copy = remote(sq_own.at[l], sq_pair.at[l], sp_ss.at[l], sp_rs.at[l], buddy)
-        sp_copy.start()
         for i in range(0, chips, 2):
             res = out_pair(i, other)
             part[i] = res[:, :LANES]
             part[i + 1] = res[:, LANES:]
+        sp_copy.wait_recv()
+        sq_send[l] = sq_own[l] + sq_pair[l]
+        for m in far:
+            remote(
+                sq_send.at[l], sq_recv.at[l, chip], sq_ss, sq_rs, 2 * chip_of[m] + other
+            ).start()
 
         def rs_copy(i):
             return remote(
-                rs_send.at[l, i], rs_recv.at[l, chip], rs_ss.at[l], rs_rs.at[l], 2 * chip_of[far[i]] + other
+                rs_send.at[l, i], rs_recv.at[l, chip], rs_ss, rs_rs, 2 * chip_of[far[i]] + other
             )
 
         for q in range(4):
@@ -560,17 +550,15 @@
             for i in range(q * quarter, (q + 1) * quarter):
                 rs_send[l, i] = (part[i] + pair_recv[l, i].astype(F32)).astype(BF16)
                 rs_copy(i).start()
-        sp_copy.wait_recv()
-        sq_send[l] = sq_own[l] + sq_pair[l]
-        for m in far:
-            remote(
-                sq_send.at[l], sq_recv.at[l, chip], sq_ss.at[l], sq_rs.at[l], 2 * chip_of[m] + other
-            ).start()
         if l + 1 < layers:
             for copy in big[l + 1]:
                 copy.start()
         update_range(l, 0, groups8)
-        remote(sq_recv.at[l], sq_recv.at[l], sq_ss.at[l], sq_rs.at[l], buddy).wait_recv()
+        sent(keys_recv.at[l, pl.ds(0, n - 1)], key_ss)
+        sent(sq_own.at[l], sp_ss)
+        sent(pair_send.at[l], pair_ss)
+        sent(sq_recv.at[l], sq_ss)
+        remote(sq_recv.at[l], sq_recv.at[l], sq_ss, sq_rs, buddy).wait_recv()
         rows = []
         for g in range(GROUPS):
             total = sq_recv[l, per_group * g]
@@ -585,7 +573,7 @@
             resid = tokens[:, pl.ds(pl.multiple_of(me * LANES, LANES), LANES)]
         else:
             resid = hidden[l - 1, me]
-        remote(rs_recv.at[l], rs_recv.at[l], rs_ss.at[l], rs_rs.at[l], buddy).wait_recv()
+        remote(rs_recv.at[l], rs_recv.at[l], rs_ss, rs_rs, buddy).wait_recv()
         sums = [resid.astype(F32)] + [jnp.zeros((batch, LANES), F32)] * 3
         for g in range(GROUPS):
             term = rs_recv[l, per_group * g].astype(F32)
@@ -595,25 +583,18 @@
         hidden[l, me] = ((sums[0] + sums[1]) + (sums[2] + sums[3])).astype(BF16)
         for m in far:
             remote(
-                hidden.at[l, me], hidden.at[l, me], ag_ss.at[l], ag_rs.at[l, m], 2 * chip_of[m] + other
+                hidden.at[l, me], hidden.at[l, me], ag_ss, ag_rs.at[wave_of[m]], 2 * chip_of[m] + other
             ).start()
 
-    forward_all(layers - 1, near)
-    whole(layers - 1, near)
+    for q in range(4):
+        forward_wave(layers - 1, q)
+    for q in range(4):
+        whole(layers - 1, q)
     for j in range(n):
         tokens_out[:, j * LANES : (j + 1) * LANES] = hidden[layers - 1, j]
-    for l in range(layers):
-        def sent(src, sem):
-            remote(src, src, sem, rs_rs.at[l], buddy).wait_send()
-
-        sent(keys_recv.at[l, pl.ds(0, n - 1)], key_ss.at[l])
-        for q in range(4):
-            sent(pair_send.at[l, pl.ds(0, chips // 4)], pair_ss.at[l, q])
-        sent(sq_own.at[l], sp_ss.at[l])
-        sent(sq_recv.at[l], sq_ss.at[l])
-        sent(rs_send.at[l], rs_ss.at[l])
-        sent(hidden.at[l, pl.ds(0, chips)], ag_ss.at[l])
-        sent(hidden.at[l, pl.ds(0, chips - 1)], fw_ss.at[l])
+    sent(rs_send.at[layers - 1], rs_ss)
+    sent(blocks(layers - 1, chips), ag_ss)
+    sent(blocks(layers - 1, chips - 1), fw_ss)
 
 
 def flush(tokens, state, value, key, tokens_hbm, state_hbm, value_hbm, key_hbm, sems):
@@ -682,22 +663,12 @@
             pltpu.VMEM((batch, entries, chans), BF16),
             pltpu.VMEM((chans, LANES), F32),
             pltpu.VMEM((batch, entries), F32),
-            dma((10,)),
-            dma((layers, 7)),
-            dma((layers,)),
-            dma((layers,)),
-            dma((layers, 4)),
-            dma((layers, 4)),
-            dma((layers,)),
-            dma((layers,)),
-            dma((layers,)),
-            dma((layers,)),
-            dma((layers,)),
-            dma((layers,)),
-            dma((layers,)),
-            dma((layers, chips)),
-            dma((layers,)),
-            dma((layers, chips)),
+            dma((17,)),
+            dma((7,)),
+            dma((4,)),
+            dma((4,)),
+            dma((4,)),
+            dma((4,)),
         ],
         compiler_params=pltpu.CompilerParams(
             collective_id=0,

time: 49.2 us -> 46.9 us (0.953)
  Pallas kernels: 48.4 us -> 46.1 us
    pallas_call x1, Pallas kernels: 44.8 us -> 42.5 us  [fused(): pl.pallas_call(functools.partial(mixer, n), out_shape=tuple((pltpu.VMEM(o...]
where the time goes in v2:
time: 46.9 us; the launch traced here: 46.7 us
  Pallas kernels  46.1 us (98%)
  between operations  0.65 us (1%)
    pallas_call x1, Pallas kernels, fused(): pl.pallas_call(functools.partial(mixer, n), out_shape=tuple((pltpu.VMEM(o...  42.5 us
    pallas_call x1, Pallas kernels, fused(): pl.pallas_call(flush, out_shape=outs, in_specs=[pl.BlockSpec(memory_space...  3.57 us

profile of v2, /device:TPU:0, one launch (start us, length us, event | category | flops | bytes accessed | tf_op | source)
XLA Modules:
  0.0 46.7 jit_solution(334333793545760643)
XLA Ops:
  0.6 42.5 %mixer.1 = (bf16[32,4096]{1,0:T(8,128)(2,1)S(1)}, f32[2,32,256,128]{3,2,1,0:T(8,128)S(1)}, f32[2,32,2,256]{3,2,1,0:T(2,128)S(1)}, f32[2,32,2,2,32]{4,3,2,1,0:T(2,128)S(1)}) custom-call(bf16[32,4096]{1,0:T(8,128)(2,1)} %tokens_hbm.1, f32[2,4096]{1,0:T(2,128)} %gain_hbm.1, bf16[2,4096,256]{2,1,0:T(8,128)(2,1)} %wg_hbm.1, bf16[2,4096,256]{2,1,0:T(8,128)(2,1)} %wv_hbm.1, ...), custom_call_target="tpu_custom_call" | custom-call | tf_op jit(solution)/shard_map/mixer/pallas_call | solution.py:642
  43.2 3.6 %flush.1 = (bf16[32,4096]{1,0:T(8,128)(2,1)}, f32[2,32,256,128]{3,2,1,0:T(8,128)}, f32[2,32,2,256]{3,2,1,0:T(2,128)}, f32[2,32,2,2,32]{4,3,2,1,0:T(2,128)}) custom-call(bf16[32,4096]{1,0:T(8,128)(2,1)S(1)} %get-tuple-element.8.tokens, f32[2,32,256,128]{3,2,1,0:T(8,128)S(1)} %get-tuple-element.9.state, f32[2,32,2,256]{3,2,1,0:T(2,128)S(1)} %get-tuple-element.10.value, ...), custom_call_target="tpu_custom_call" | custom-call | tf_op jit(solution)/shard_map/flush/pallas_call | solution.py:680

commit v3 on v2

--- a/solution.py
+++ b/solution.py
@@ -258,8 +258,8 @@
     def distance(m):
         return (m >> 2) + (m >> 1) % 2 + m % 2
 
-    near = sorted(range(chips), key=lambda m: (distance(m), m))
-    far = near[::-1]
+    far = sorted(range(chips), key=lambda m: (-distance(m), m))
+    near = far[::-1]
 
     barrier = pltpu.get_barrier_semaphore()
 
@@ -281,14 +281,11 @@
             device_id_type=pl.DeviceIdType.MESH,
         )
 
-    row = iota((2 * LANES, 2 * entries), 0)
-    col = iota((2 * LANES, 2 * entries), 1)
-    half = row // LANES
-    inner = row % LANES
-    entry = half * 2 + inner // (LANES // 2)
-    sender = (inner % (LANES // 2)) // 2
-    recv_hot = jnp.where(
-        col == (inner % 2) * entries + sender * own_entries + entry, 1.0, 0.0
+    senders = entries // own_entries
+    row = iota((entries, entries), 0)
+    col = iota((entries, entries), 1)
+    natural = jnp.where(
+        col == (row % senders) * own_entries + row // senders, 1.0, 0.0
     ).astype(BF16)
     row = iota((heads, chans), 0)
     col = iota((heads, chans), 1)
@@ -458,32 +455,28 @@
             sent(blocks(l - 1, chips - 1), fw_ss)
 
         def turn(g, carry):
-            for j in range(4):
-                turned[4 * g + j] = state[l, 4 * g + j].T.astype(BF16)
+            for j in range(8):
+                turned[8 * g + j] = lax.dot_general(
+                    natural, state[l, 8 * g + j].astype(BF16), NT, preferred_element_type=F32
+                ).astype(BF16)
             return carry
 
-        lax.fori_loop(0, batch // 4, turn, 0)
+        lax.fori_loop(0, groups8, turn, 0)
         big[l][6].wait()
 
         remote(
             keys_recv.at[l, pl.ds(0, n - 1)], keys_recv.at[l, pl.ds(0, n - 1)],
             key_ss, key_rs, buddy,
         ).wait_recv()
-        arrived = keys_recv[l].reshape(2 * n, LANES)
-        arrived = jnp.concatenate([arrived, arrived], axis=0).T
-        left_half = iota((batch, LANES), 1) < LANES // 2
-        pieces = [
-            jnp.where(
-                left_half,
-                arrived[2 * h * batch : (2 * h + 1) * batch],
-                arrived[(2 * h + 1) * batch : (2 * h + 2) * batch],
-            )
-            for h in range(2)
-        ]
-        both = select_dot(jnp.concatenate(pieces, axis=1), recv_hot)
-        writes = both[:, :entries]
-        reads = both[:, entries:]
-        wbuf[...] = writes
+        lane_entry = iota((batch, LANES), 1) // senders
+        grouped = []
+        for i in range(2):
+            arrived = jnp.concatenate([keys_recv[l, :, i, :]] * own_entries, axis=0).T
+            rows = arrived[:batch]
+            for e in range(1, own_entries):
+                rows = jnp.where(lane_entry == e, arrived[e * batch : (e + 1) * batch], rows)
+            grouped.append(rows)
+        writes, reads = grouped
         lane_half = iota((8, 2 * entries), 1) // entries
         sub = iota((8, 2 * entries), 0)
         query = []
@@ -553,6 +546,7 @@
         if l + 1 < layers:
             for copy in big[l + 1]:
                 copy.start()
+        wbuf[...] = select_dot(writes, natural)
         update_range(l, 0, groups8)
         sent(keys_recv.at[l, pl.ds(0, n - 1)], key_ss)
         sent(sq_own.at[l], sp_ss)

time: 46.9 us -> 45.6 us (0.972)
  Pallas kernels: 46.1 us -> 44.8 us
    pallas_call x1, Pallas kernels: 42.5 us -> 41.3 us  [fused(): pl.pallas_call(functools.partial(mixer, n), out_shape=tuple((pltpu.VMEM(o...]
where the time goes in v3:
time: 45.6 us; the launch traced here: 45.5 us
  Pallas kernels  44.8 us (98%)
  between operations  0.65 us (1%)
    pallas_call x1, Pallas kernels, fused(): pl.pallas_call(functools.partial(mixer, n), out_shape=tuple((pltpu.VMEM(o...  41.3 us
    pallas_call x1, Pallas kernels, fused(): pl.pallas_call(flush, out_shape=outs, in_specs=[pl.BlockSpec(memory_space...  3.57 us

profile of v3, /device:TPU:0, one launch (start us, length us, event | category | flops | bytes accessed | tf_op | source)
XLA Modules:
  0.0 45.5 jit_solution(16446012447000462565)
XLA Ops:
  0.6 41.3 %mixer.1 = (bf16[32,4096]{1,0:T(8,128)(2,1)S(1)}, f32[2,32,256,128]{3,2,1,0:T(8,128)S(1)}, f32[2,32,2,256]{3,2,1,0:T(2,128)S(1)}, f32[2,32,2,2,32]{4,3,2,1,0:T(2,128)S(1)}) custom-call(bf16[32,4096]{1,0:T(8,128)(2,1)} %tokens_hbm.1, f32[2,4096]{1,0:T(2,128)} %gain_hbm.1, bf16[2,4096,256]{2,1,0:T(8,128)(2,1)} %wg_hbm.1, bf16[2,4096,256]{2,1,0:T(8,128)(2,1)} %wv_hbm.1, ...), custom_call_target="tpu_custom_call" | custom-call | tf_op jit(solution)/shard_map/mixer/pallas_call | solution.py:636
  41.9 3.6 %flush.1 = (bf16[32,4096]{1,0:T(8,128)(2,1)}, f32[2,32,256,128]{3,2,1,0:T(8,128)}, f32[2,32,2,256]{3,2,1,0:T(2,128)}, f32[2,32,2,2,32]{4,3,2,1,0:T(2,128)}) custom-call(bf16[32,4096]{1,0:T(8,128)(2,1)S(1)} %get-tuple-element.8.tokens, f32[2,32,256,128]{3,2,1,0:T(8,128)S(1)} %get-tuple-element.9.state, f32[2,32,2,256]{3,2,1,0:T(2,128)S(1)} %get-tuple-element.10.value, ...), custom_call_target="tpu_custom_call" | custom-call | tf_op jit(solution)/shard_map/flush/pallas_call | solution.py:674

commit v4 on v3

--- a/solution.py
+++ b/solution.py
@@ -241,9 +241,6 @@
         ]
         for l in range(layers)
     ]
-    for copy in small[:4] + big[0][:2]:
-        copy.start()
-
     def flipped(value, mask):
         bit = 1
         out = value
@@ -266,7 +263,12 @@
     def signal(to):
         pl.semaphore_signal(barrier, inc=1, device_id=(to,), device_id_type=pl.DeviceIdType.MESH)
 
-    for m in far[:-1]:
+    for m in far[:4]:
+        signal(2 * chip_of[m])
+        signal(2 * chip_of[m] + 1)
+    for copy in small[:4] + big[0][:2]:
+        copy.start()
+    for m in far[4:-1]:
         signal(2 * chip_of[m])
         signal(2 * chip_of[m] + 1)
     signal(buddy)
@@ -605,7 +607,7 @@
             copies.append(
                 pltpu.make_async_copy(state.at[l, at], state_hbm.at[l, at], sems.at[len(copies)])
             )
-    for copy in copies:
+    for copy in copies[3:] + copies[:3]:
         copy.start()
     for copy in copies:
         copy.wait()

time: 45.6 us -> 45.6 us (level)
  no operation moved by 1% of the time
where the time goes in v4:
time: 45.6 us; the launch traced here: 45.5 us
  Pallas kernels  44.8 us (98%)
  between operations  0.65 us (1%)
    pallas_call x1, Pallas kernels, fused(): pl.pallas_call(functools.partial(mixer, n), out_shape=tuple((pltpu.VMEM(o...  41.3 us
    pallas_call x1, Pallas kernels, fused(): pl.pallas_call(flush, out_shape=outs, in_specs=[pl.BlockSpec(memory_space...  3.54 us

profile of v4, /device:TPU:0, one launch (start us, length us, event | category | flops | bytes accessed | tf_op | source)
XLA Modules:
  0.0 45.5 jit_solution(11518191769192342092)
XLA Ops:
  0.6 41.3 %mixer.1 = (bf16[32,4096]{1,0:T(8,128)(2,1)S(1)}, f32[2,32,256,128]{3,2,1,0:T(8,128)S(1)}, f32[2,32,2,256]{3,2,1,0:T(2,128)S(1)}, f32[2,32,2,2,32]{4,3,2,1,0:T(2,128)S(1)}) custom-call(bf16[32,4096]{1,0:T(8,128)(2,1)} %tokens_hbm.1, f32[2,4096]{1,0:T(2,128)} %gain_hbm.1, bf16[2,4096,256]{2,1,0:T(8,128)(2,1)} %wg_hbm.1, bf16[2,4096,256]{2,1,0:T(8,128)(2,1)} %wv_hbm.1, ...), custom_call_target="tpu_custom_call" | custom-call | tf_op jit(solution)/shard_map/mixer/pallas_call | solution.py:638
  41.9 3.5 %flush.1 = (bf16[32,4096]{1,0:T(8,128)(2,1)}, f32[2,32,256,128]{3,2,1,0:T(8,128)}, f32[2,32,2,256]{3,2,1,0:T(2,128)}, f32[2,32,2,2,32]{4,3,2,1,0:T(2,128)}) custom-call(bf16[32,4096]{1,0:T(8,128)(2,1)S(1)} %get-tuple-element.8.tokens, f32[2,32,256,128]{3,2,1,0:T(8,128)S(1)} %get-tuple-element.9.state, f32[2,32,2,256]{3,2,1,0:T(2,128)S(1)} %get-tuple-element.10.value, ...), custom_call_target="tpu_custom_call" | custom-call | tf_op jit(solution)/shard_map/flush/pallas_call | solution.py:676
